TPU v7x, 32 devices: a whole 2x2x4 slice. The times are simulated.
32 devices in a mesh: sp: 8 (over z, x), tp: 4 (over y, core).
Axes of the slice: x: 2, y: 2, z: 4, core: 2. Of those that a mesh axis runs over, the one named last changes fastest.
Arguments:
- cotangent: bfloat16 [1536, 2048], P('sp'), may hold values from -8 to 8
- residual: bfloat16 [1536, 2048], P('sp'), may hold values from -6 to 6
- norm_gain: float32 [2048], replicated, may hold values from 0.1 to 1.9
- route_ids: int32 [1536, 2], P('sp'), may hold values from 0 to 7, all different within a row; in each aligned block of 192 rows (0 to 191, 192 to 383, ...) at most 96 rows name the same one
- route_weights: float32 [1536, 2], P('sp'), may hold values from 0.1 to 1
- expert_gate: bfloat16 [8, 2048, 1024], P('sp', None, 'tp'), may hold values from -0.125 to 0.125
- expert_up: bfloat16 [8, 2048, 1024], P('sp', None, 'tp'), may hold values from -0.125 to 0.125
- expert_down: bfloat16 [8, 1024, 2048], P('sp', 'tp'), may hold values from -0.1875 to 0.1875
- out_proj: bfloat16 [2048, 1024], P(None, 'tp'), may hold values from -0.1875 to 0.1875
- conv_out: bfloat16 [1536, 1024], P('sp', 'tp'), may hold values from -6 to 6, as said below
- branch_gate: bfloat16 [1536, 1024], P('sp', 'tp'), may hold values from -6 to 6
- prev_state: bfloat16 [1536, 1024], P('sp', 'tp'), may hold values from -6 to 6
- decay_param: float32 [1024], P('tp'), as said below
- rate_map: bfloat16 [16, 64, 64], P('tp'), may hold values from -0.75 to 0.75
- input_map: bfloat16 [16, 64, 64], P('tp'), may hold values from -0.75 to 0.75
Outputs:
- grad_gate: float32 [8, 2048, 1024], P('sp', None, 'tp')
- grad_up: float32 [8, 2048, 1024], P('sp', None, 'tp')
- grad_down: float32 [8, 1024, 2048], P('sp', 'tp')
- grad_out_proj: float32 [2048, 1024], P('sp', 'tp')
- grad_conv_out: float32 [1536, 1024], P('sp', 'tp')
- grad_branch_gate: float32 [1536, 1024], P('sp', 'tp')
Inputs may be any that keep to these rules, and one draw needn't show every extreme that they name: `route_ids`: within the rows of one device (aligned blocks of 192 rows) no expert is named by more than 96 rows, a bound that some block reaches; the two ids of a row differ. `conv_out`: every entry is a finite value between -6 and 6. `decay_param`: every channel's decay parameter is at least 4.
All inputs are finite; a program needn't handle non-finite values.
Results may differ from a plain program's by a relative error of at most 0.0095.
Values may be sent and summed in bfloat16 or wider, within the bound.
A program may use at most 128 MiB of HBM per device.

v0:
```python
import jax
import jax.numpy as jnp
from jax import lax
from jax.sharding import PartitionSpec as P

RATE_SCALE = 8.0
NORM_EPS = 1e-06
SERIES_EDGE = 0.001


def entering(part, axis, combine, identity):
    count = lax.axis_size(axis)
    place = lax.axis_index(axis)
    ahead = count - 1 - place
    gathered = jax.tree.map(lambda a: lax.all_gather(a, axis), part)
    state = jax.tree.map(lambda a, e: jnp.zeros_like(a) + jnp.asarray(e, a.dtype), part, identity)

    def one(turn, state):
        source = count - 1 - turn
        return combine(
            state, jax.tree.map(lambda a: lax.dynamic_index_in_dim(a, source, 0, False), gathered)
        )

    return lax.fori_loop(0, ahead, one, state)


def gelu_pair(values):
    result, pullback = jax.vjp(jax.nn.gelu, values)
    return (result, pullback(jnp.ones_like(values))[0])


def gate_maps(conv_out, weights):
    rows_here = conv_out.shape[0]
    blocked = conv_out.reshape(rows_here, weights.shape[0], weights.shape[1])
    mapped = jnp.einsum("tbi,bij->tbj", blocked, weights, preferred_element_type=jnp.float32)
    return mapped.reshape(rows_here, -1)


def gate_maps_back(grad_values, weights):
    rows_here = grad_values.shape[0]
    blocked = grad_values.reshape(rows_here, weights.shape[0], weights.shape[2])
    mapped = jnp.einsum(
        "tbj,bij->tbi", blocked, weights.astype(jnp.float32), precision=lax.Precision.HIGHEST
    )
    return mapped.reshape(rows_here, -1)


def norm_slope(spread):
    tiny_side = spread < SERIES_EDGE
    denominator = jnp.where(tiny_side, 1.0, -jnp.expm1(-spread))
    series_ratio = jnp.where(tiny_side, 1.0 + 0.5 * spread, spread / denominator)
    return 0.5 * jnp.sqrt(spread * series_ratio)


def reverse_linear(factors, term_values):

    def combine(left_pair, right_pair):
        return (left_pair[0] * right_pair[0], right_pair[0] * left_pair[1] + right_pair[1])

    flipped = lax.associative_scan(
        combine, (jnp.flip(factors, 0), jnp.flip(term_values, 0)), axis=0
    )
    return jnp.flip(flipped[1], 0)


def per_device(
    cotangent,
    residual,
    norm_gain,
    route_ids,
    route_weights,
    expert_gate,
    expert_up,
    expert_down,
    out_proj,
    conv_out,
    branch_gate,
    prev_state,
    decay_param,
    rate_map,
    input_map,
):
    tok_rows, model_width = residual.shape
    sp_count = lax.axis_size("sp")
    tp_count = lax.axis_size("tp")
    local_experts = expert_gate.shape[0]
    experts_all = local_experts * sp_count
    capacity = 4 * tok_rows // experts_all
    slot_total = experts_all * capacity
    res_values = residual.astype(jnp.float32)
    inv_rms = lax.rsqrt(jnp.mean(res_values * res_values, axis=1, keepdims=True) + NORM_EPS)
    moe_input = (res_values * inv_rms * norm_gain[None, :]).astype(jnp.bfloat16)
    scaled_cot = (route_weights[:, :, None] * cotangent.astype(jnp.float32)[:, None, :]).astype(
        jnp.bfloat16
    )
    scaled_cot = scaled_cot.reshape(2 * tok_rows, model_width)
    flat_ids = route_ids.reshape(-1)
    expert_hits = (flat_ids[:, None] == jnp.arange(experts_all, dtype=jnp.int32)[None, :]).astype(
        jnp.int32
    )
    earlier_hits = jnp.cumsum(expert_hits, axis=0) - expert_hits
    slot_pos = flat_ids * capacity + jnp.sum(earlier_hits * expert_hits, axis=1)
    slot_match = slot_pos[None, :] == jnp.arange(slot_total, dtype=jnp.int32)[:, None]
    source_row = jnp.sum(
        jnp.where(slot_match, jnp.arange(2 * tok_rows, dtype=jnp.int32)[None, :], 0), axis=1
    )
    filled = jnp.any(slot_match, axis=1)
    cot_send = jnp.where(filled[:, None], scaled_cot[source_row], jnp.zeros((), jnp.bfloat16))
    cot_send = cot_send.reshape(experts_all, capacity, model_width)
    rows_send = moe_input[source_row // 2].reshape(experts_all, capacity, model_width)
    part_cols = model_width // tp_count
    col_start = lax.axis_index("tp") * part_cols
    cot_part = lax.dynamic_slice_in_dim(cot_send, col_start, part_cols, 2)
    rows_part = lax.dynamic_slice_in_dim(rows_send, col_start, part_cols, 2)
    cot_part, rows_part = (
        lax.all_to_all(cot_part, "sp", split_axis=0, concat_axis=0, tiled=True),
        lax.all_to_all(rows_part, "sp", split_axis=0, concat_axis=0, tiled=True),
    )
    cot_recv, rows_recv = (
        lax.all_gather(cot_part, "tp", axis=2, tiled=True),
        lax.all_gather(rows_part, "tp", axis=2, tiled=True),
    )

    def to_expert_rows(slots):
        shaped = slots.reshape(sp_count, local_experts, capacity, slots.shape[2])
        return jnp.transpose(shaped, (1, 0, 2, 3)).reshape(
            local_experts, sp_count * capacity, slots.shape[2]
        )

    rows_in = to_expert_rows(rows_recv)
    cot_in = to_expert_rows(cot_recv)
    gate_pre = jnp.einsum("erd,edf->erf", rows_in, expert_gate, preferred_element_type=jnp.float32)
    up_pre = jnp.einsum("erd,edf->erf", rows_in, expert_up, preferred_element_type=jnp.float32)
    gate_sig = jax.nn.sigmoid(gate_pre)
    gate_act = gate_pre * gate_sig
    hidden = (gate_act * up_pre).astype(jnp.bfloat16)
    d_hidden = jnp.einsum("erd,efd->erf", cot_in, expert_down, preferred_element_type=jnp.float32)
    d_up = (d_hidden * gate_act).astype(jnp.bfloat16)
    d_gate = (d_hidden * up_pre * gate_sig * (1.0 + gate_pre * (1.0 - gate_sig))).astype(
        jnp.bfloat16
    )
    grad_down = jnp.einsum("erf,erd->efd", hidden, cot_in, preferred_element_type=jnp.float32)
    grad_gate = jnp.einsum("erd,erf->edf", rows_in, d_gate, preferred_element_type=jnp.float32)
    grad_up = jnp.einsum("erd,erf->edf", rows_in, d_up, preferred_element_type=jnp.float32)
    back_terms = jnp.einsum("erf,edf->erd", d_gate, expert_gate, preferred_element_type=jnp.float32)
    back_terms = back_terms + jnp.einsum(
        "erf,edf->erd", d_up, expert_up, preferred_element_type=jnp.float32
    )
    back_terms = back_terms.astype(jnp.bfloat16)
    back_terms = jnp.transpose(
        back_terms.reshape(local_experts, sp_count, capacity, model_width), (1, 0, 2, 3)
    )
    back_terms = back_terms.reshape(sp_count * local_experts, capacity, model_width)
    summed = (
        lax.psum_scatter(back_terms, "tp", scatter_dimension=2, tiled=True)
        .astype(jnp.float32)
        .astype(jnp.bfloat16)
    )
    returned = lax.all_to_all(summed, "sp", split_axis=0, concat_axis=0, tiled=True)
    returned = lax.all_gather(returned, "tp", axis=2, tiled=True)
    back_rows = returned.reshape(slot_total, model_width)[slot_pos].astype(jnp.float32)
    d_normed = jnp.sum(back_rows.reshape(tok_rows, 2, model_width), axis=1)
    weighted = norm_gain[None, :] * d_normed
    cubed = inv_rms * inv_rms * inv_rms
    d_mix = (
        cotangent.astype(jnp.float32)
        + inv_rms * weighted
        - res_values * cubed * jnp.mean(res_values * weighted, axis=1, keepdims=True)
    ).astype(jnp.bfloat16)
    rate_gate = jax.nn.sigmoid(gate_maps(conv_out, rate_map))
    input_gate = jax.nn.sigmoid(gate_maps(conv_out, input_map))
    soft_decay = jax.nn.softplus(-decay_param)
    log_keep = -RATE_SCALE * rate_gate * soft_decay[None, :]
    keep_rate = jnp.exp(log_keep)
    spread = -2.0 * log_keep
    norm_term = jnp.sqrt(-jnp.expm1(-spread))
    conv_values = conv_out.astype(jnp.float32)
    prev_values = prev_state.astype(jnp.float32)
    state_now = keep_rate * prev_values + norm_term * input_gate * conv_values
    gelu_value, gelu_slope = gelu_pair(branch_gate.astype(jnp.float32))
    branch_out = (state_now * gelu_value).astype(jnp.bfloat16)
    grad_out_proj = lax.psum_scatter(
        lax.dot_general(
            d_mix, branch_out, (((0,), (0,)), ((), ())), preferred_element_type=jnp.float32
        ),
        "sp",
        scatter_dimension=0,
        tiled=True,
    )
    d_branch = jnp.dot(d_mix, out_proj, preferred_element_type=jnp.float32)
    next_keep = jnp.concatenate([keep_rate[1:], jnp.zeros_like(keep_rate[:1])], axis=0)
    local_grad = reverse_linear(next_keep, d_branch * gelu_value)
    next_log = jnp.concatenate([log_keep[1:], jnp.zeros_like(log_keep[:1])], axis=0)
    tail_keep = jnp.exp(jnp.flip(jnp.cumsum(jnp.flip(next_log, 0), axis=0), 0))
    block_keep = jnp.exp(jnp.sum(log_keep, axis=0))
    head_term = keep_rate[0] * local_grad[0]

    def compose(earlier, later_part):
        return (later_part[0] * earlier[0], later_part[0] * earlier[1] + later_part[1])

    carried = entering(
        (block_keep, head_term),
        "sp",
        compose,
        (jnp.ones_like(block_keep), jnp.zeros_like(head_term)),
    )
    state_grad = local_grad + tail_keep * carried[1][None, :]
    grad_branch_gate = d_branch * state_now * gelu_slope
    keep_grad = state_grad * prev_values * keep_rate
    inner_input = input_gate * conv_values
    rate_back = keep_grad * (-RATE_SCALE * soft_decay[None, :]) * rate_gate * (1.0 - rate_gate)
    rate_back = rate_back + state_grad * inner_input * keep_rate * keep_rate * (
        1.0 - rate_gate
    ) * norm_slope(spread)
    input_back = state_grad * norm_term * conv_values * input_gate * (1.0 - input_gate)
    grad_conv_out = (
        state_grad * norm_term * input_gate
        + gate_maps_back(rate_back, rate_map)
        + gate_maps_back(input_back, input_map)
    )
    return (grad_gate, grad_up, grad_down, grad_out_proj, grad_conv_out, grad_branch_gate)


def solution(mesh):
    in_specs = (
        P("sp", None),
        P("sp", None),
        P(),
        P("sp", None),
        P("sp", None),
        P("sp", None, "tp"),
        P("sp", None, "tp"),
        P("sp", "tp", None),
        P(None, "tp"),
        P("sp", "tp"),
        P("sp", "tp"),
        P("sp", "tp"),
        P("tp"),
        P("tp", None, None),
        P("tp", None, None),
    )
    out_specs = (
        P("sp", None, "tp"),
        P("sp", None, "tp"),
        P("sp", "tp", None),
        P("sp", "tp"),
        P("sp", "tp"),
        P("sp", "tp"),
    )
    return jax.shard_map(
        per_device, mesh=mesh, in_specs=in_specs, out_specs=out_specs, check_vma=False
    )
```

profile of v0, /device:TPU:0, one launch (start us, length us, event | category | flops | bytes accessed | tf_op | source)
XLA Modules:
  0.0 328.5 jit_solution(5379476029609607391)
XLA Ops:
  12.7 4.2 %gather_fusion = bf16[768,2048]{1,0:T(8,128)(2,1)} fusion(bf16[192,2048]{1,0:T(8,128)(2,1)S(1)} %fusion.2, s32[1024]{0:T(1024)S(1)} %get-tuple-element.138), kind=kCustom, calls=%fused_computation | custom fusion | bytes 6294528 | tf_op jit(solution)/shard_map/gather | solution.py:110
  18.2 27.3 %all_to_all.15 = bf16[8,96,512]{2,1,0:T(8,128)(2,1)} all-to-all(bf16[8,96,512]{2,1,0:T(8,128)(2,1)S(1)} %constant_dynamic-slice_fusion.2), channel_id=1, replica_groups=mesh['sp'=8,'tp'=4] {'sp'}, dimensions={0} | all-to-all | bytes 1572864 | tf_op jit(solution)/shard_map/all_to_all | solution.py:117
  45.6 3.3 mul.385
  48.9 5.5 %mul.386 = f32[384,2048]{1,0:T(8,128)} reshape(f32[192,2,2048]{2,1,0:T(2,128)} %mul.385) | data formatting | bytes 6291456 | tf_op jit(solution)/shard_map/mul | solution.py:93
  55.0 2.1 multiply_convert_fusion
  57.1 4.3 %gather_fusion.1 = bf16[768,2048]{1,0:T(8,128)(2,1)} fusion(bf16[384,2048]{1,0:T(8,128)(2,1)S(1)} %multiply_convert_fusion, s32[1024]{0:T(1024)S(1)} %get-tuple-element.137), kind=kCustom, calls=%fused_computation.1 | custom fusion | bytes 6294528 | tf_op jit(solution)/shard_map/gather | solution.py:108
  62.8 23.6 %all_to_all.16 = bf16[8,96,512]{2,1,0:T(8,128)(2,1)} all-to-all(bf16[8,96,512]{2,1,0:T(8,128)(2,1)S(1)} %dynamic-slice_select_fusion), channel_id=1, replica_groups=mesh['sp'=8,'tp'=4] {'sp'}, dimensions={0} | all-to-all | bytes 1572864 | tf_op jit(solution)/shard_map/all_to_all | solution.py:116
  86.5 3.0 fusion.16
  89.7 1.9 fusion.19
  91.6 22.6 %all-gather.8.cloned.1.call-done = bf16[8,96,2048]{2,1,0:T(8,128)(2,1)} async-done(((bf16[8,96,512]{2,1,0:T(8,128)(2,1)}), bf16[8,96,2048]{2,1,0:T(8,128)(2,1)}) %all-gather.8.cloned.1.call-update) | async-done | bytes 3145744 | tf_op jit(solution)/shard_map/all_gather | solution.py:120
  114.1 3.6 %multiply_convert_fusion.2 = (bf16[768,256]{1,0:T(8,128)(2,1)S(1)}, bf16[768,256]{1,0:T(8,128)(2,1)S(1)}) fusion(f32[768,256]{1,0:T(8,128)S(1)} %fusion.16, f32[768,256]{1,0:T(8,128)} %fusion.19, bf16[768,2048]{1,0:T(8,128)(2,1)} %bitcast.126, bf16[1,256,2048]{2,1,0:T(8,128)(2,1)} %param.24), kind=kOutput, calls=%fused_computation.44 | convolution fusion | flops 807862272 | bytes 6553600 | tf_op jit(solution)/shard_map/erd,efd->erf/dot_general | solution.py:137
  118.8 2.7 add_convert_fusion
  121.6 37.8 %reduce-scatter.3.cloned.1.call-done = bf16[8,96,512]{2,1,0:T(8,128)(2,1)} async-done(((bf16[8,96,2048]{2,1,0:T(8,128)(2,1)}), bf16[8,96,512]{2,1,0:T(8,128)(2,1)}) %reduce-scatter.3.cloned.1.call-update) | async-done | bytes 786448 | tf_op jit(solution)/shard_map/reduce_scatter | solution.py:155
  159.4 25.6 %all_to_all.17 = bf16[8,96,512]{2,1,0:T(8,128)(2,1)} all-to-all(bf16[8,96,512]{2,1,0:T(8,128)(2,1)} %reduce-scatter.3.cloned.1.call-done), channel_id=1, replica_groups=mesh['sp'=8,'tp'=4] {'sp'}, dimensions={0} | all-to-all | bytes 1572864 | tf_op jit(solution)/shard_map/all_to_all | solution.py:159
  190.3 18.6 %all-gather = f32[8,1,256]{2,1,0:T(1,128)S(1)} all-gather(f32[1,1,256]{2,1,0:T(1,128)S(1)} %reshape.345), channel_id=1, replica_groups=mesh['sp'=8,'tp'=4] {'sp'}, dimensions={0}, use_global_device_ids=true | all-gather | bytes 9216 | tf_op jit(solution)/shard_map/all_gather | solution.py:15
  211.8 6.7 %gather_fusion.2 = bf16[384,2048]{1,0:T(8,128)(2,1)S(1)} fusion(bf16[768,2048]{1,0:T(8,128)(2,1)} %bitcast.99, s32[1024]{0:T(1024)S(1)} %pad_clamp_fusion), kind=kCustom, calls=%fused_computation.2 | custom fusion | bytes 3147264 | tf_op jit(solution)/shard_map/gather | solution.py:161
  218.5 3.4 %reshape.320 = f32[192,2,2048]{2,1,0:T(2,128)} reshape(bf16[384,2048]{1,0:T(8,128)(2,1)S(1)} %gather_fusion.2) | data formatting | bytes 4718592 | tf_op jit(solution)/shard_map/convert_element_type | solution.py:161
  221.8 5.7 %reduce_sum.63 = f32[192,2048]{1,0:T(8,128)S(1)} reduce(f32[192,2,2048]{2,1,0:T(2,128)} %reshape.320, f32[]{:T(128)} %constant.89.clone.1), dimensions={1}, to_apply=%region_7.8 | reduce | flops 393216 | bytes 4718596 | tf_op jit(solution)/shard_map/reduce_sum | solution.py:162
  232.8 20.5 %all-gather.1 = f32[8,1,256]{2,1,0:T(1,128)S(1)} all-gather(f32[1,1,256]{2,1,0:T(1,128)S(1)} %fusion.71), channel_id=1, replica_groups=mesh['sp'=8,'tp'=4] {'sp'}, dimensions={0}, use_global_device_ids=true | all-gather | bytes 9216 | tf_op jit(solution)/shard_map/all_gather | solution.py:15
  255.2 1.9 fusion.50
  257.1 4.4 %convolution_bitcast_fusion.2 = f32[1,2048,256]{2,1,0:T(8,128)} fusion(bf16[768,2048]{1,0:T(8,128)(2,1)} %bitcast.123, bf16[768,256]{1,0:T(8,128)(2,1)S(1)} %copy-done.7), kind=kOutput, calls=%fused_computation.14 | convolution fusion | flops 805306368 | bytes 5636096 | tf_op jit(solution)/shard_map/erd,erf->edf/dot_general | solution.py:143
  261.5 2.4 convolution_bitcast_fusion.1
  264.6 2.4 convolution_bitcast_fusion
  268.8 53.2 %reduce-scatter.5.cloned.1.call-done = f32[256,256]{1,0:T(8,128)} async-done(((f32[2048,256]{1,0:T(8,128)}), f32[256,256]{1,0:T(8,128)}) %reduce-scatter.5.cloned.1.call-update) | async-done | bytes 262160 | tf_op jit(solution)/shard_map/reduce_scatter | solution.py:182
  (254 shorter events, 27.1 us)
Async XLA Ops:
  7.2 79.4 %copy-start = (bf16[1,2048,256]{2,1,0:T(8,128)(2,1)S(1)}, bf16[1,2048,256]{2,1,0:T(8,128)(2,1)}, u32[]{:S(2)}) copy-start(bf16[1,2048,256]{2,1,0:T(8,128)(2,1)} %param.22) | copy-start | bytes 3145732
  7.2 79.3 %all-gather.6.cloned.1.call-start = ((), (), s32[]{:S(2)}) async-start(), calls=%async_computation.5 | async-start | bytes 3932160 | tf_op jit(solution)/shard_map/all_gather | solution.py:121
  16.9 28.7 %copy-start.3 = (bf16[192,2048]{1,0:T(8,128)(2,1)S(1)}, bf16[192,2048]{1,0:T(8,128)(2,1)}, u32[]{:S(2)}) copy-start(bf16[192,2048]{1,0:T(8,128)(2,1)} %param.17) | copy-start | bytes 2359300
  45.5 68.6 %all-gather.8.cloned.1.call-start = ((), (), s32[]{:S(2)}) async-start(), calls=%async_computation.6 | async-start | bytes 3932160 | tf_op jit(solution)/shard_map/all_gather | solution.py:120
  48.9 5.5 %copy-start.27 = (f32[192,2]{0,1:T(2,128)S(1)}, f32[192,2]{0,1:T(2,128)}, u32[]{:S(2)}) copy-start(f32[192,2]{0,1:T(2,128)} %param.21) | copy-start | bytes 4612
  86.4 73.0 %reduce-scatter.3.cloned.1.call-start = ((), (), s32[]{:S(2)}) async-start(), calls=%async_computation.7 | async-start | bytes 3932160 | tf_op jit(solution)/shard_map/reduce_scatter | solution.py:155
  86.5 3.2 copy-start.29
  89.7 24.5 %copy-start.32 = (f32[768,256]{1,0:T(8,128)}, f32[768,256]{1,0:T(8,128)S(1)}, u32[]{:S(2)}) copy-start(f32[768,256]{1,0:T(8,128)S(1)} %fusion.16) | copy-start | bytes 2359300
  121.5 63.8 %copy-start.13 = (bf16[192,256]{1,0:T(8,128)(2,1)S(1)}, bf16[192,256]{1,0:T(8,128)(2,1)}, u32[]{:S(2)}) copy-start(bf16[192,256]{1,0:T(8,128)(2,1)} %param.26) | copy-start | bytes 294916
  121.5 63.9 %copy-start.28 = (f32[256]{0:T(256)S(1)}, f32[256]{0:T(256)}, u32[]{:S(2)}) copy-start(f32[256]{0:T(256)} %param.29) | copy-start | bytes 3076
  121.5 64.0 %copy-start.24 = (bf16[4,64,64]{2,1,0:T(8,128)(2,1)S(1)}, bf16[4,64,64]{2,1,0:T(8,128)(2,1)}, u32[]{:S(2)}) copy-start(bf16[4,64,64]{2,1,0:T(8,128)(2,1)} %param.30) | copy-start | bytes 98308
  121.6 90.2 %all-gather.10.cloned.1.call-start = ((), (), s32[]{:S(2)}) async-start(), calls=%async_computation.8 | async-start | bytes 3932160 | tf_op jit(solution)/shard_map/all_gather | solution.py:160
  185.0 136.9 %reduce-scatter.5.cloned.1.call-start = ((), (), s32[]{:S(2)}) async-start(), calls=%async_computation.9 | async-start | bytes 2359296 | tf_op jit(solution)/shard_map/reduce_scatter | solution.py:182
  221.8 5.7 %copy-start.2 = (bf16[192,2048]{1,0:T(8,128)(2,1)S(1)}, bf16[192,2048]{1,0:T(8,128)(2,1)}, u32[]{:S(2)}) copy-start(bf16[192,2048]{1,0:T(8,128)(2,1)} %param.18) | copy-start | bytes 2359300
  221.8 5.7 %copy-start.21 = (f32[2048]{0:T(1024)S(1)}, f32[2048]{0:T(1024)}, u32[]{:S(2)}) copy-start(f32[2048]{0:T(1024)} %param.19) | copy-start | bytes 24580
  231.3 22.6 %copy-start.5 = (f32[192,256]{1,0:T(8,128)S(1)}, f32[192,256]{1,0:T(8,128)}, u32[]{:S(2)}) copy-start(f32[192,256]{1,0:T(8,128)} %copy.89) | copy-start | bytes 589828
  231.3 22.6 %copy-start.12 = (f32[192,256]{1,0:T(8,128)S(1)}, f32[192,256]{1,0:T(8,128)}, u32[]{:S(2)}) copy-start(f32[192,256]{1,0:T(8,128)} %rev.14) | copy-start | bytes 589828
  231.3 22.6 %copy-start.14 = (bf16[192,256]{1,0:T(8,128)(2,1)S(1)}, bf16[192,256]{1,0:T(8,128)(2,1)}, u32[]{:S(2)}) copy-start(bf16[192,256]{1,0:T(8,128)(2,1)} %param.26) | copy-start | bytes 294916
  231.3 22.6 %copy-start.20 = (bf16[192,256]{1,0:T(8,128)(2,1)S(1)}, bf16[192,256]{1,0:T(8,128)(2,1)}, u32[]{:S(2)}) copy-start(bf16[192,256]{1,0:T(8,128)(2,1)} %param.28) | copy-start | bytes 294916
  257.1 4.4 %copy-start.19 = (bf16[768,256]{1,0:T(8,128)(2,1)S(1)}, bf16[768,256]{1,0:T(8,128)(2,1)}, u32[]{:S(2)}) copy-start(bf16[768,256]{1,0:T(8,128)(2,1)} %copy-done.18) | copy-start | bytes 1179652
  257.1 4.4 %copy-start.30 = (bf16[8,96,2048]{2,1,0:T(8,128)(2,1)S(1)}, bf16[8,96,2048]{2,1,0:T(8,128)(2,1)}, u32[]{:S(2)}) copy-start(bf16[8,96,2048]{2,1,0:T(8,128)(2,1)} %all-gather.6.cloned.1.call-done) | copy-start | bytes 9437188
  261.5 3.1 copy-start.34
  264.6 3.1 copy-start.25
  264.6 57.4 %copy-start.1 = (bf16[1,2048,256]{2,1,0:T(8,128)(2,1)S(1)}, bf16[1,2048,256]{2,1,0:T(8,128)(2,1)}, u32[]{:S(2)}) copy-start(bf16[1,2048,256]{2,1,0:T(8,128)(2,1)} %param.22) | copy-start | bytes 3145732
  (16 other events, 26.1 us)
Sparse Core Ops, SparseCore 0:
  45.7 27.5 all-gather.5
  86.6 27.5 all-gather.7
  121.7 37.7 reduce-scatter.2
  185.1 26.5 all-gather.9
  257.2 64.6 reduce-scatter.4
where the time goes:
time: 329 us; the launch traced here: 328 us
  blocking collectives  116 us (35%)
  waiting for transfers between devices  114 us (35%)
  local copies, waits for them, and re-layouts  40.5 us (12%)
  matrix products  24.8 us (8%)
  other arithmetic  17.6 us (5%)
  between operations  14.9 us (5%)
    reduce_scatter x1, waiting for transfers between devices, per_device(): lax.psum_scatter(lax.dot_general(d_mix, branch_out, (((0,), (0,)), ((), (...  53.2 us
    all_gather x2, blocking collectives, entering(): gathered = jax.tree.map(lambda a: lax.all_gather(a, axis), part)  39.1 us
    reduce_scatter x1, waiting for transfers between devices, per_device(): lax.psum_scatter(back_terms, 'tp', scatter_dimension=2, tiled=True)  37.8 us
    all_to_all x1, blocking collectives, per_device(): lax.all_to_all(rows_part, 'sp', split_axis=0, concat_axis=0, tiled=True)  27.3 us
    all_to_all x1, blocking collectives, per_device(): lax.all_to_all(summed, 'sp', split_axis=0, concat_axis=0, tiled=True)  25.6 us
    all_to_all x1, blocking collectives, per_device(): lax.all_to_all(cot_part, 'sp', split_axis=0, concat_axis=0, tiled=True)  23.6 us
    all_gather x1, waiting for transfers between devices, per_device(): lax.all_gather(cot_part, 'tp', axis=2, tiled=True)  22.6 us
    mul x3, local copies, waits for them, and re-layouts, per_device(): route_weights[:, :, None] * cotangent.astype(jnp.float32)[:, None, :]  8.95 us
  transfers between devices with their start and end apart: 5, of which 4 were waited for; matrix products, arithmetic and copies ran while one was open for 12% of the time, Pallas kernels for 0%

commit v1 on v0

--- a/solution.py
+++ b/solution.py
@@ -117,7 +117,9 @@
         lax.all_to_all(rows_part, "sp", split_axis=0, concat_axis=0, tiled=True),
     )
     cot_recv, rows_recv = (
-        lax.all_gather(cot_part, "tp", axis=2, tiled=True),
+        jnp.concatenate(
+            lax.all_to_all(jnp.stack([cot_part] * lax.axis_size("tp")), "tp", 0, 0), axis=2
+        ),
         lax.all_gather(rows_part, "tp", axis=2, tiled=True),
     )
 

time: 329 us -> 348 us (1.058)
  blocking collectives: 116 us -> 155 us
  waiting for transfers between devices: 114 us -> 89.7 us
  local copies, waits for them, and re-layouts: 40.5 us -> 46.9 us
    all_to_all x0 -> x1, blocking collectives: none -> 39.5 us  [per_device(): lax.all_to_all(jnp.stack([cot_part] * lax.axis_size('tp')), 'tp', 0, 0)]
    all_gather x1 -> x0, waiting for transfers between devices: 22.6 us -> none  [per_device(): lax.all_gather(cot_part, 'tp', axis=2, tiled=True)]
    unnamed x77 -> x82, local copies, waits for them, and re-layouts: 3.8 us -> 7.4 us
  transfers between devices with their start and end apart: 5 -> 4, of which waited for: 4 -> 3; matrix products, arithmetic and copies ran while one was open for 12% -> 11% of each run, Pallas kernels for 0% -> 0%
where the time goes in v1:
time: 348 us
  blocking collectives  155 us (45%)
  waiting for transfers between devices  89.7 us (26%)
  local copies, waits for them, and re-layouts  46.9 us (13%)
  matrix products  21.5 us (6%)
  other arithmetic  18.8 us (5%)
  between operations  14.9 us (4%)
    reduce_scatter x1, waiting for transfers between devices, per_device(): lax.psum_scatter(lax.dot_general(d_mix, branch_out, (((0,), (0,)), ((), (...  53.2 us
    all_to_all x1, blocking collectives, per_device(): lax.all_to_all(jnp.stack([cot_part] * lax.axis_size('tp')), 'tp', 0, 0)  39.5 us
    all_gather x2, blocking collectives, entering(): gathered = jax.tree.map(lambda a: lax.all_gather(a, axis), part)  39.3 us
    reduce_scatter x1, waiting for transfers between devices, per_device(): lax.psum_scatter(back_terms, 'tp', scatter_dimension=2, tiled=True)  35.9 us
    all_to_all x1, blocking collectives, per_device(): lax.all_to_all(rows_part, 'sp', split_axis=0, concat_axis=0, tiled=True)  27.3 us
    all_to_all x1, blocking collectives, per_device(): lax.all_to_all(summed, 'sp', split_axis=0, concat_axis=0, tiled=True)  25.6 us
    all_to_all x1, blocking collectives, per_device(): lax.all_to_all(cot_part, 'sp', split_axis=0, concat_axis=0, tiled=True)  23.5 us
    mul x3, local copies, waits for them, and re-layouts, per_device(): route_weights[:, :, None] * cotangent.astype(jnp.float32)[:, None, :]  8.95 us
  transfers between devices with their start and end apart: 4, of which 3 were waited for; matrix products, arithmetic and copies ran while one was open for 11% of the time, Pallas kernels for 0%

profile of v1, /device:TPU:0, one launch (start us, length us, event | category | flops | bytes accessed | tf_op | source)
XLA Modules:
  0.0 347.7 jit_solution(3609740321477224040)
XLA Ops:
  12.7 4.2 %gather_fusion = bf16[768,2048]{1,0:T(8,128)(2,1)} fusion(bf16[192,2048]{1,0:T(8,128)(2,1)S(1)} %fusion.2, s32[1024]{0:T(1024)S(1)} %get-tuple-element.138), kind=kCustom, calls=%fused_computation | custom fusion | bytes 6294528 | tf_op jit(solution)/shard_map/gather | solution.py:110
  18.2 27.3 %all_to_all.20 = bf16[8,96,512]{2,1,0:T(8,128)(2,1)} all-to-all(bf16[8,96,512]{2,1,0:T(8,128)(2,1)S(1)} %constant_dynamic-slice_fusion.2), channel_id=1, replica_groups=mesh['sp'=8,'tp'=4] {'sp'}, dimensions={0} | all-to-all | bytes 1572864 | tf_op jit(solution)/shard_map/all_to_all | solution.py:117
  45.6 3.3 mul.385
  48.9 5.5 %mul.386 = f32[384,2048]{1,0:T(8,128)} reshape(f32[192,2,2048]{2,1,0:T(2,128)} %mul.385) | data formatting | bytes 6291456 | tf_op jit(solution)/shard_map/mul | solution.py:93
  55.0 2.1 multiply_convert_fusion
  57.1 4.3 %gather_fusion.1 = bf16[768,2048]{1,0:T(8,128)(2,1)} fusion(bf16[384,2048]{1,0:T(8,128)(2,1)S(1)} %multiply_convert_fusion, s32[1024]{0:T(1024)S(1)} %get-tuple-element.137), kind=kCustom, calls=%fused_computation.1 | custom fusion | bytes 6294528 | tf_op jit(solution)/shard_map/gather | solution.py:108
  62.8 23.5 %all_to_all.21 = bf16[8,96,512]{2,1,0:T(8,128)(2,1)S(1)} all-to-all(bf16[8,96,512]{2,1,0:T(8,128)(2,1)S(1)} %dynamic-slice_select_fusion), channel_id=1, replica_groups=mesh['sp'=8,'tp'=4] {'sp'}, dimensions={0} | all-to-all | bytes 1572864 | tf_op jit(solution)/shard_map/all_to_all | solution.py:116
  86.7 39.5 %all_to_all.22 = bf16[4,8,96,512]{3,2,1,0:T(8,128)(2,1)S(1)} all-to-all(bf16[4,8,96,512]{3,2,1,0:T(8,128)(2,1)S(1)} %stack.2), channel_id=1, replica_groups=mesh['sp'=8,'tp'=4] {'tp'}, dimensions={0} | all-to-all | bytes 6291456 | tf_op jit(solution)/shard_map/all_to_all | solution.py:121
  126.2 2.4 copy.85
  128.6 2.7 copy.108
  131.3 3.0 fusion.16
  139.5 2.7 add_convert_fusion
  142.3 35.9 %reduce-scatter.3.cloned.1.call-done = bf16[8,96,512]{2,1,0:T(8,128)(2,1)} async-done(((bf16[8,96,2048]{2,1,0:T(8,128)(2,1)}), bf16[8,96,512]{2,1,0:T(8,128)(2,1)}) %reduce-scatter.3.cloned.1.call-update) | async-done | bytes 786448 | tf_op jit(solution)/shard_map/reduce_scatter | solution.py:157
  178.2 25.6 %all_to_all.23 = bf16[8,96,512]{2,1,0:T(8,128)(2,1)} all-to-all(bf16[8,96,512]{2,1,0:T(8,128)(2,1)} %reduce-scatter.3.cloned.1.call-done), channel_id=1, replica_groups=mesh['sp'=8,'tp'=4] {'sp'}, dimensions={0} | all-to-all | bytes 1572864 | tf_op jit(solution)/shard_map/all_to_all | solution.py:161
  208.9 18.8 %all-gather = f32[8,1,256]{2,1,0:T(1,128)S(1)} all-gather(f32[1,1,256]{2,1,0:T(1,128)S(1)} %reshape.351), channel_id=1, replica_groups=mesh['sp'=8,'tp'=4] {'sp'}, dimensions={0}, use_global_device_ids=true | all-gather | bytes 9216 | tf_op jit(solution)/shard_map/all_gather | solution.py:15
  230.6 6.7 %gather_fusion.2 = bf16[384,2048]{1,0:T(8,128)(2,1)S(1)} fusion(bf16[768,2048]{1,0:T(8,128)(2,1)} %bitcast.102, s32[1024]{0:T(1024)S(1)} %pad_clamp_fusion), kind=kCustom, calls=%fused_computation.2 | custom fusion | bytes 3147264 | tf_op jit(solution)/shard_map/gather | solution.py:163
  237.3 3.4 reshape.326
  240.7 5.7 %reduce_sum.63 = f32[192,2048]{1,0:T(8,128)S(1)} reduce(f32[192,2,2048]{2,1,0:T(2,128)} %reshape.326, f32[]{:T(128)} %constant.89.clone.1), dimensions={1}, to_apply=%region_7.8 | reduce | flops 393216 | bytes 4718596 | tf_op jit(solution)/shard_map/reduce_sum | solution.py:164
  252.0 20.5 %all-gather.1 = f32[8,1,256]{2,1,0:T(1,128)S(1)} all-gather(f32[1,1,256]{2,1,0:T(1,128)S(1)} %fusion.71), channel_id=1, replica_groups=mesh['sp'=8,'tp'=4] {'sp'}, dimensions={0}, use_global_device_ids=true | all-gather | bytes 9216 | tf_op jit(solution)/shard_map/all_gather | solution.py:15
  274.4 1.9 fusion.50
  276.3 4.4 %convolution_bitcast_fusion.2 = f32[1,2048,256]{2,1,0:T(8,128)} fusion(bf16[768,2048]{1,0:T(8,128)(2,1)} %bitcast.130, bf16[768,256]{1,0:T(8,128)(2,1)S(1)} %copy-done.8), kind=kOutput, calls=%fused_computation.14 | convolution fusion | flops 805306368 | bytes 5636096 | tf_op jit(solution)/shard_map/erd,erf->edf/dot_general | solution.py:145
  280.7 2.4 convolution_bitcast_fusion.1
  283.8 2.4 convolution_bitcast_fusion
  287.9 53.2 %reduce-scatter.5.cloned.1.call-done = f32[256,256]{1,0:T(8,128)} async-done(((f32[2048,256]{1,0:T(8,128)}), f32[256,256]{1,0:T(8,128)}) %reduce-scatter.5.cloned.1.call-update) | async-done | bytes 262160 | tf_op jit(solution)/shard_map/reduce_scatter | solution.py:184
  (259 shorter events, 31.5 us)
Async XLA Ops:
  7.2 124.1 %copy-start = (bf16[1,2048,256]{2,1,0:T(8,128)(2,1)S(1)}, bf16[1,2048,256]{2,1,0:T(8,128)(2,1)}, u32[]{:S(2)}) copy-start(bf16[1,2048,256]{2,1,0:T(8,128)(2,1)} %param.22) | copy-start | bytes 3145732
  7.2 124.1 %all-gather.5.cloned.1.call-start = ((), (), s32[]{:S(2)}) async-start(), calls=%async_computation.6 | async-start | bytes 3932160 | tf_op jit(solution)/shard_map/all_gather | solution.py:123
  16.9 28.7 %copy-start.5 = (bf16[192,2048]{1,0:T(8,128)(2,1)S(1)}, bf16[192,2048]{1,0:T(8,128)(2,1)}, u32[]{:S(2)}) copy-start(bf16[192,2048]{1,0:T(8,128)(2,1)} %param.17) | copy-start | bytes 2359300
  45.5 132.7 %reduce-scatter.3.cloned.1.call-start = ((), (), s32[]{:S(2)}) async-start(), calls=%async_computation.7 | async-start | bytes 3932160 | tf_op jit(solution)/shard_map/reduce_scatter | solution.py:157
  48.9 5.5 %copy-start.28 = (f32[192,2]{0,1:T(2,128)S(1)}, f32[192,2]{0,1:T(2,128)}, u32[]{:S(2)}) copy-start(f32[192,2]{0,1:T(2,128)} %param.21) | copy-start | bytes 4612
  131.3 3.2 copy-start.30
  134.4 4.0 %copy-start.33 = (f32[768,256]{1,0:T(8,128)}, f32[768,256]{1,0:T(8,128)S(1)}, u32[]{:S(2)}) copy-start(f32[768,256]{1,0:T(8,128)S(1)} %fusion.16) | copy-start | bytes 2359300
  142.2 61.6 %copy-start.14 = (bf16[192,256]{1,0:T(8,128)(2,1)S(1)}, bf16[192,256]{1,0:T(8,128)(2,1)}, u32[]{:S(2)}) copy-start(bf16[192,256]{1,0:T(8,128)(2,1)} %param.26) | copy-start | bytes 294916
  142.2 61.8 %copy-start.29 = (f32[256]{0:T(256)S(1)}, f32[256]{0:T(256)}, u32[]{:S(2)}) copy-start(f32[256]{0:T(256)} %param.29) | copy-start | bytes 3076
  142.2 61.9 %copy-start.25 = (bf16[4,64,64]{2,1,0:T(8,128)(2,1)S(1)}, bf16[4,64,64]{2,1,0:T(8,128)(2,1)}, u32[]{:S(2)}) copy-start(bf16[4,64,64]{2,1,0:T(8,128)(2,1)} %param.30) | copy-start | bytes 98308
  142.3 63.2 %copy-start.27 = (s32[192,2]{0,1:T(2,128)S(1)}, s32[192,2]{0,1:T(2,128)}, u32[]{:S(2)}) copy-start(s32[192,2]{0,1:T(2,128)} %param.20) | copy-start | bytes 4612
  142.3 63.5 %copy-start.23 = (bf16[4,64,64]{2,1,0:T(8,128)(2,1)S(1)}, bf16[4,64,64]{2,1,0:T(8,128)(2,1)}, u32[]{:S(2)}) copy-start(bf16[4,64,64]{2,1,0:T(8,128)(2,1)} %param.31) | copy-start | bytes 98308
  142.3 88.3 %all-gather.7.cloned.1.call-start = ((), (), s32[]{:S(2)}) async-start(), calls=%async_computation.8 | async-start | bytes 3932160 | tf_op jit(solution)/shard_map/all_gather | solution.py:162
  203.8 137.3 %reduce-scatter.5.cloned.1.call-start = ((), (), s32[]{:S(2)}) async-start(), calls=%async_computation.9 | async-start | bytes 2359296 | tf_op jit(solution)/shard_map/reduce_scatter | solution.py:184
  240.6 5.7 %copy-start.2 = (bf16[192,2048]{1,0:T(8,128)(2,1)S(1)}, bf16[192,2048]{1,0:T(8,128)(2,1)}, u32[]{:S(2)}) copy-start(bf16[192,2048]{1,0:T(8,128)(2,1)} %param.18) | copy-start | bytes 2359300
  240.7 5.7 %copy-start.22 = (f32[2048]{0:T(1024)S(1)}, f32[2048]{0:T(1024)}, u32[]{:S(2)}) copy-start(f32[2048]{0:T(1024)} %param.19) | copy-start | bytes 24580
  249.4 23.6 %copy-start.6 = (f32[192,256]{1,0:T(8,128)S(1)}, f32[192,256]{1,0:T(8,128)}, u32[]{:S(2)}) copy-start(f32[192,256]{1,0:T(8,128)} %copy.91) | copy-start | bytes 589828
  249.5 23.6 %copy-start.13 = (f32[192,256]{1,0:T(8,128)S(1)}, f32[192,256]{1,0:T(8,128)}, u32[]{:S(2)}) copy-start(f32[192,256]{1,0:T(8,128)} %rev.14) | copy-start | bytes 589828
  249.5 23.6 %copy-start.15 = (bf16[192,256]{1,0:T(8,128)(2,1)S(1)}, bf16[192,256]{1,0:T(8,128)(2,1)}, u32[]{:S(2)}) copy-start(bf16[192,256]{1,0:T(8,128)(2,1)} %param.26) | copy-start | bytes 294916
  249.5 23.6 %copy-start.21 = (bf16[192,256]{1,0:T(8,128)(2,1)S(1)}, bf16[192,256]{1,0:T(8,128)(2,1)}, u32[]{:S(2)}) copy-start(bf16[192,256]{1,0:T(8,128)(2,1)} %param.28) | copy-start | bytes 294916
  276.3 4.4 %copy-start.20 = (bf16[768,256]{1,0:T(8,128)(2,1)S(1)}, bf16[768,256]{1,0:T(8,128)(2,1)}, u32[]{:S(2)}) copy-start(bf16[768,256]{1,0:T(8,128)(2,1)} %copy-done.19) | copy-start | bytes 1179652
  276.3 4.4 %copy-start.31 = (bf16[8,96,2048]{2,1,0:T(8,128)(2,1)S(1)}, bf16[8,96,2048]{2,1,0:T(8,128)(2,1)}, u32[]{:S(2)}) copy-start(bf16[8,96,2048]{2,1,0:T(8,128)(2,1)} %all-gather.5.cloned.1.call-done) | copy-start | bytes 9437188
  280.7 3.1 copy-start.36
  283.8 57.4 %copy-start.1 = (bf16[1,2048,256]{2,1,0:T(8,128)(2,1)S(1)}, bf16[1,2048,256]{2,1,0:T(8,128)(2,1)}, u32[]{:S(2)}) copy-start(bf16[1,2048,256]{2,1,0:T(8,128)(2,1)} %param.22) | copy-start | bytes 3145732
  (17 other events, 34.0 us)
Sparse Core Ops, SparseCore 0:
  45.7 27.5 all-gather.4
  142.4 35.7 reduce-scatter.2
  203.9 26.5 all-gather.6
  276.4 64.7 reduce-scatter.4
